TPU v7x, 32 devices: a whole 2x2x4 slice. The times are simulated.
32 devices in a mesh: ep: 8 (over z, y), tp: 4 (over x, core).
Axes of the slice: x: 2, y: 2, z: 4, core: 2. Of those that a mesh axis runs over, the one named last changes fastest.
Arguments:
- queries_a: bfloat16 [1024, 1024], P('ep', 'tp'), may hold values from -128 to 128
- queries_b: bfloat16 [1024, 1024], P('ep', 'tp'), may hold values from -128 to 128
- keys_a: bfloat16 [1024, 512], P('ep', 'tp'), may hold values from -8 to 8
- keys_b: bfloat16 [1024, 512], P('ep', 'tp'), may hold values from -8 to 8
- values: bfloat16 [1024, 1024], P('ep', 'tp'), may hold values from -6 to 6
- lambdas: float32 [16], P('tp'), may hold values from 0.3 to 0.8
- head_gain: float32 [128], replicated, may hold values from 0.1 to 1.9
- w_out: bfloat16 [2048, 2048], P('tp'), may hold values from -0.125 to 0.125
- moe_tokens: bfloat16 [4096, 2048], P(('ep', 'tp')), may hold values from -80 to 80
- moe_gain: float32 [2048], replicated, may hold values from 0.1 to 1.9
- routes: int32 [4096, 2], P(('ep', 'tp')), may hold values from 0 to 7, all different within a row; in each aligned block of 128 rows (0 to 127, 128 to 255, ...) at most 48 rows name the same one
- route_weights: float32 [4096, 2], P(('ep', 'tp')), may hold values from 0.1 to 1
- w_gate: bfloat16 [8, 2048, 2048], P('ep', None, 'tp'), may hold values from -4 to 4
- w_up: bfloat16 [8, 2048, 2048], P('ep', None, 'tp'), may hold values from -4 to 4
- w_down: bfloat16 [8, 2048, 2048], P('ep', 'tp'), may hold values from -0.0625 to 0.0625
Outputs:
- mixer_out: bfloat16 [1024, 2048], P(('ep', 'tp'))
- moe_out: bfloat16 [4096, 2048], P(('ep', 'tp'))
Inputs may be any that keep to these rules, and one draw needn't show every extreme that they name: `routes`: each row names 2 different experts. Within the rows of one device no expert is named by more than 48 rows, a bound that some block reaches of some device.
All inputs are finite; a program needn't handle non-finite values.
Results may differ from a plain program's by a relative error of at most 0.011.
Values may be sent and summed in bfloat16 or wider, within the bound.
A program may use at most 192 MiB of HBM per device.

v0:
```python
import jax
import jax.numpy as jnp
from jax import lax
from jax.sharding import PartitionSpec as P

HEAD = 64
VDIM = 128
TOP = 2
eps = 1e-05
alpha_act = 1.702
limit_act = 7.0
negative = -1e30


def clamped_unit(gate, up):
    capped = jnp.minimum(gate, limit_act)
    linear = jnp.clip(up, -limit_act, limit_act)
    return capped * jax.nn.sigmoid(alpha_act * capped) * (linear + 1.0)


def hidden_rows(inputs, gate_matrix, up_matrix):
    gate = jnp.dot(inputs, gate_matrix, preferred_element_type=jnp.float32)
    up = jnp.dot(inputs, up_matrix, preferred_element_type=jnp.float32)
    return clamped_unit(gate, up).astype(jnp.bfloat16)


def pick_rows(table, owner):
    valid = owner < table.shape[0]
    chosen = jnp.take(table, jnp.minimum(owner, table.shape[0] - 1), axis=0)
    return jnp.where(valid[:, None], chosen, jnp.zeros_like(chosen))


def mixer(queries_a, queries_b, keys_a, keys_b, values, lambdas, head_gain, w_out):
    tokens = queries_a.shape[0]
    local_heads = lambdas.shape[0]
    kv_local = keys_a.shape[1] // HEAD
    group = local_heads // kv_local
    scale = HEAD ** (-0.5)
    query_pos = lax.axis_index("ep") * tokens + jnp.arange(tokens, dtype=jnp.int32)
    grouped_a = queries_a.reshape(tokens, kv_local, group, HEAD)
    grouped_b = queries_b.reshape(tokens, kv_local, group, HEAD)
    lowest = jnp.full((kv_local, group, tokens), negative, jnp.float32)
    nothing = jnp.zeros((kv_local, group, tokens), jnp.float32)
    blank = jnp.zeros((kv_local, group, tokens, VDIM), jnp.float32)

    def one_map(grouped, keys, value_rows, visible, state):
        peak, total, accum = state
        scores = (
            jnp.einsum("rgjd,ngd->gjrn", grouped, keys, preferred_element_type=jnp.float32) * scale
        )
        scores = jnp.where(visible, scores, negative)
        new_peak = jnp.maximum(peak, jnp.max(scores, axis=-1))
        expo = jnp.where(visible, jnp.exp(scores - new_peak[..., None]), 0.0)
        total = jnp.sum(expo, axis=-1)
        accum = jnp.einsum(
            "gjrn,ngv->gjrv",
            expo.astype(jnp.bfloat16),
            value_rows,
            preferred_element_type=jnp.float32,
        )
        return (new_peak, total, accum)

    initial = (lowest, nothing, blank, lowest, nothing, blank)
    piece_a = lax.all_gather(keys_a, "ep", axis=0, tiled=True)
    piece_b = lax.all_gather(keys_b, "ep", axis=0, tiled=True)
    piece_v = lax.all_gather(values, "ep", axis=0, tiled=True)
    count = piece_a.shape[0]

    def visit(state):
        key_pos = jnp.arange(count, dtype=jnp.int32)
        visible = key_pos[None, :] <= query_pos[:, None]
        value_rows = piece_v.reshape(count, kv_local, VDIM)
        first = one_map(
            grouped_a, piece_a.reshape(count, kv_local, HEAD), value_rows, visible, state[:3]
        )
        second = one_map(
            grouped_b, piece_b.reshape(count, kv_local, HEAD), value_rows, visible, state[3:]
        )
        return first + second

    result = lax.cond(jnp.int32(0) <= query_pos[tokens - 1], visit, lambda state: state, initial)
    mixed_a = result[2] / result[1][..., None]
    mixed_b = result[5] / result[4][..., None]
    diff = mixed_a - lambdas.reshape(kv_local, group, 1, 1) * mixed_b
    heads_out = (
        diff * lax.rsqrt(jnp.mean(diff * diff, axis=-1, keepdims=True) + eps) * head_gain
    ).astype(jnp.bfloat16)
    weights_out = w_out.reshape(kv_local, group, VDIM, w_out.shape[1])
    return lax.psum_scatter(
        jnp.einsum(
            "gjrv,gjvd->rd", heads_out, weights_out, preferred_element_type=jnp.float32
        ).astype(jnp.bfloat16),
        "tp",
        scatter_dimension=0,
        tiled=True,
    )


def experts(moe_tokens, moe_gain, routes, route_weights, w_gate, w_up, w_down):
    tok_rows, width = moe_tokens.shape
    n_experts = lax.axis_size("ep") * w_gate.shape[0]
    capacity = max(2, 3 * tok_rows * TOP // (2 * n_experts))
    inputs = moe_tokens.astype(jnp.float32)
    normed = (
        inputs * lax.rsqrt(jnp.mean(inputs * inputs, axis=-1, keepdims=True) + eps) * moe_gain
    ).astype(jnp.bfloat16)
    chosen = routes.reshape(-1)
    member = (chosen[:, None] == jnp.arange(n_experts, dtype=jnp.int32)[None, :]).astype(jnp.int32)
    order_in = jnp.sum(jnp.cumsum(member, axis=0) * member, axis=1) - 1
    slot_ids = chosen * capacity + order_in
    owner = (
        jnp.full((n_experts * capacity,), tok_rows, jnp.int32)
        .at[slot_ids]
        .set(jnp.arange(tok_rows * TOP, dtype=jnp.int32) // TOP)
    )
    outgoing = pick_rows(normed, owner).reshape(n_experts, capacity, width)
    arrived = lax.all_to_all(outgoing, "ep", split_axis=0, concat_axis=1, tiled=True).reshape(
        -1, width
    )
    hidden = hidden_rows(lax.all_gather(arrived, "tp", axis=0, tiled=True), w_gate[0], w_up[0])
    expert_out = lax.psum_scatter(
        jnp.dot(hidden, w_down[0], preferred_element_type=jnp.float32).astype(jnp.bfloat16),
        "tp",
        scatter_dimension=0,
        tiled=True,
    )
    returned = lax.all_to_all(
        expert_out.reshape(-1, capacity, width), "ep", split_axis=0, concat_axis=0, tiled=True
    )
    picked = jnp.take(returned.reshape(-1, width), slot_ids, axis=0).reshape(tok_rows, TOP, width)
    return jnp.sum(picked.astype(jnp.float32) * route_weights[:, :, None], axis=1).astype(
        jnp.bfloat16
    )


def body(
    queries_a,
    queries_b,
    keys_a,
    keys_b,
    values,
    lambdas,
    head_gain,
    w_out,
    moe_tokens,
    moe_gain,
    routes,
    route_weights,
    w_gate,
    w_up,
    w_down,
):
    mixer_out = mixer(queries_a, queries_b, keys_a, keys_b, values, lambdas, head_gain, w_out)
    moe_out = experts(moe_tokens, moe_gain, routes, route_weights, w_gate, w_up, w_down)
    return (mixer_out, moe_out)


def solution(mesh):
    return jax.shard_map(
        body,
        mesh=mesh,
        in_specs=(
            P("ep", "tp"),
            P("ep", "tp"),
            P("ep", "tp"),
            P("ep", "tp"),
            P("ep", "tp"),
            P("tp"),
            P(),
            P("tp", None),
            P(("ep", "tp"), None),
            P(),
            P(("ep", "tp"), None),
            P(("ep", "tp"), None),
            P("ep", None, "tp"),
            P("ep", None, "tp"),
            P("ep", "tp", None),
        ),
        out_specs=(P(("ep", "tp"), None), P(("ep", "tp"), None)),
        check_vma=False,
    )
```

profile of v0, /device:TPU:0, one launch (start us, length us, event | category | flops | bytes accessed | tf_op | source)
XLA Modules:
  0.0 350.4 jit_solution(3916929698931288925)
XLA Ops:
  7.2 0.9 copy.49
  8.2 0.1 eq.26
  8.3 0.1 reshape.159
  8.4 0.7 broadcast_multiply_fusion
  9.1 0.6 reduce-window.6
  9.7 0.2 slice_reduce_fusion
  10.0 0.1 fusion.34
  10.1 0.1 copy.53
  10.2 0.1 mul.117
  10.3 1.4 scatter_custom_fusion
  12.0 1.2 fusion.27
  13.2 1.2 fusion.29
  14.5 3.1 gather_fusion
  17.6 1.7 select_select_fusion
  19.3 44.2 %all_to_all.14 = bf16[8,48,2048]{2,1,0:T(8,128)(2,1)} all-to-all(bf16[8,48,2048]{2,1,0:T(8,128)(2,1)S(1)} %select_select_fusion), channel_id=1, replica_groups=mesh['ep'=8,'tp'=4] {'ep'}, dimensions={0} | all-to-all | bytes 3145728 | tf_op jit(solution)/shard_map/all_to_all | solution.py:117
  63.5 45.5 %all-gather.2.cloned.1.call-done = bf16[1536,2048]{1,0:T(8,128)(2,1)} async-done(((bf16[384,2048]{1,0:T(8,128)(2,1)}), bf16[1536,2048]{1,0:T(8,128)(2,1)}) %all-gather.2.cloned.1.call-update) | async-done | bytes 6291472 | tf_op jit(solution)/shard_map/all_gather | solution.py:120
  109.0 8.5 %convolution_minimum_fusion = f32[1536,512]{1,0:T(8,128)} fusion(bf16[1536,2048]{1,0:T(8,128)(2,1)} %all-gather.2.cloned.1.call-done, bf16[1,2048,512]{2,1,0:T(8,128)(2,1)} %param.29), kind=kOutput, calls=%fused_computation.30 | convolution fusion | flops 3222011904 | bytes 11534336 | tf_op jit(solution)/shard_map/dot_general | solution.py:22
  117.5 11.9 %convolution_convert_fusion = bf16[1536,2048]{1,0:T(8,128)(2,1)} fusion(bf16[1,512,2048]{2,1,0:T(8,128)(2,1)S(1)} %copy-done, bf16[1536,2048]{1,0:T(8,128)(2,1)} %all-gather.2.cloned.1.call-done, f32[1536,512]{1,0:T(8,128)} %convolution_minimum_fusion, bf16[1,2048,512]{2,1,0:T(8,128)(2,1)} %param.30), kind=kOutput, calls=%fused_computation.28 | convolution fusion | flops 6452674560 | bytes 19922944 | tf_op jit(solution)/shard_map/dot_general | solution.py:122
  129.5 58.9 %reduce-scatter.5.cloned.1.call-done = bf16[384,2048]{1,0:T(8,128)(2,1)} async-done(((bf16[1536,2048]{1,0:T(8,128)(2,1)}), bf16[384,2048]{1,0:T(8,128)(2,1)}) %reduce-scatter.5.cloned.1.call-update) | async-done | bytes 1572880 | tf_op jit(solution)/shard_map/reduce_scatter | solution.py:121
  188.4 5.5 %all-to-all-start.1 = ((bf16[8,48,2048]{2,1,0:T(8,128)(2,1)}), bf16[8,48,2048]{2,1,0:T(8,128)(2,1)}, u32[]{:S(2)}, u32[]{:S(2)}) async-start(bf16[8,48,2048]{2,1,0:T(8,128)(2,1)} %bitcast.77), calls=%async_computation.3 | async-start | bytes 3145728 | tf_op jit(solution)/shard_map/all_to_all | solution.py:127
  194.0 0.1 copy.45
  194.1 0.1 copy.46
  194.3 0.6 slice.9
  195.5 0.7 mul.106
  196.2 54.2 %all_gather.12 = bf16[1024,128]{0,1:T(8,128)(2,1)S(1)} all-gather(bf16[128,128]{0,1:T(8,128)(2,1)S(1)} %copy.45), channel_id=1, replica_groups=mesh['ep'=8,'tp'=4] {'ep'}, dimensions={0}, use_global_device_ids=true | all-gather | bytes 294912 | tf_op jit(solution)/shard_map/all_gather | solution.py:64
  250.3 27.8 %all_gather.14 = bf16[1024,128]{0,1:T(8,128)(2,1)} all-gather(bf16[128,128]{0,1:T(8,128)(2,1)S(1)} %copy.46), channel_id=1, replica_groups=mesh['ep'=8,'tp'=4] {'ep'}, dimensions={0}, use_global_device_ids=true | all-gather | bytes 294912 | tf_op jit(solution)/shard_map/all_gather | solution.py:65
  278.2 31.3 %all_gather.13 = bf16[1024,256]{1,0:T(8,128)(2,1)S(1)} all-gather(bf16[128,256]{1,0:T(8,128)(2,1)S(1)} %copy-done.6), channel_id=1, replica_groups=mesh['ep'=8,'tp'=4] {'ep'}, dimensions={0}, use_global_device_ids=true | all-gather | bytes 589824 | tf_op jit(solution)/shard_map/all_gather | solution.py:66
  309.5 12.2 %conditional.1 = (f32[2,2,128]{2,1,0:T(2,128)S(1)}, f32[2,2,128,128]{3,2,1,0:T(8,128)S(1)}, f32[2,2,128]{2,1,0:T(2,128)S(1)}, f32[2,2,128,128]{3,2,1,0:T(8,128)S(1)}) conditional(s32[]{:T(128)} %bitcast.12, () %tuple.16, (s32[128]{0:T(128)S(1)}, bf16[1024,128]{0,1:T(8,128)(2,1)S(1)}, bf16[128,256]{1,0:T(8,128)(2,1)}, bf16[1024,256]{1,0:T(8,128)(2,1)S(1)}, ...), branch_computations={%region_0.0_spmd, %region_1.6_spmd} | conditional | flops 416414720 | bytes 47481572 | solution.py:81
  309.5 0.1 iota_compare_fusion
  309.6 1.0 copy.47
  310.6 1.8 fusion.42
  312.4 0.1 copy.48
  312.5 2.4 fusion.1
  315.0 1.0 fusion.5
  316.0 0.2 copy-done.3
  316.3 0.1 reshape.149
  316.4 0.8 copy-done.5
  317.2 2.6 fusion.6
  319.8 1.9 fusion.8
  321.7 1.0 multiply_reduce_fusion.1
  322.7 2.9 fusion.23
  325.7 0.1 sub.35
  325.9 0.1 copy.52
  326.1 0.1 copy.54
  326.2 4.0 %gather_fusion.1 = bf16[256,2048]{1,0:T(8,128)(2,1)S(1)} fusion(bf16[384,2048]{1,0:T(8,128)(2,1)} %bitcast.26, s32[1024]{0:T(1024)S(1)} %pad_clamp_fusion), kind=kCustom, calls=%fused_computation.1 | custom fusion | bytes 2098176 | tf_op jit(solution)/shard_map/jit(_take)/gather | solution.py:130
  330.2 1.5 gather.15
  331.7 6.2 %multiply_reduce_fusion = bf16[128,2048]{1,0:T(8,128)(2,1)} fusion(bf16[128,2,2048]{2,1,0:T(2,128)(2,1)} %gather.15, pred[128,2]{1,0:T(8,128)(4,1)S(1)} %copy.52, f32[128,2]{1,0:T(8,128)S(1)} %copy.54), kind=kLoop, calls=%fused_computation.39 | loop fusion | flops 1835008 | bytes 1574144 | tf_op jit(solution)/shard_map/reduce_sum | solution.py:131
  338.0 5.9 %reduce-scatter.3.cloned.1.call-done = bf16[32,2048]{1,0:T(8,128)(2,1)} async-done(((bf16[128,2048]{1,0:T(8,128)(2,1)}), bf16[32,2048]{1,0:T(8,128)(2,1)}) %reduce-scatter.3.cloned.1.call-update) | async-done | bytes 131088 | tf_op jit(solution)/shard_map/reduce_scatter | solution.py:89
  (55 shorter events, 0.6 us)
Async XLA Ops:
  7.2 110.4 %copy-start = (bf16[1,512,2048]{2,1,0:T(8,128)(2,1)S(1)}, bf16[1,512,2048]{2,1,0:T(8,128)(2,1)}, u32[]{:S(2)}) copy-start(bf16[1,512,2048]{2,1,0:T(8,128)(2,1)} %param.31) | copy-start | bytes 6291460
  7.2 101.8 %all-gather.2.cloned.1.call-start = ((), (), s32[]{:S(2)}) async-start(), calls=%async_computation.5 | async-start | bytes 7864320 | tf_op jit(solution)/shard_map/all_gather | solution.py:120
  10.3 1.4 copy-start.12
  63.5 124.9 %reduce-scatter.5.cloned.1.call-start = ((), (), s32[]{:S(2)}) async-start(), calls=%async_computation.6 | async-start | bytes 7864320 | tf_op jit(solution)/shard_map/reduce_scatter | solution.py:121
  129.4 64.6 %copy-start.8 = (bf16[128,128]{1,0:T(8,128)(2,1)S(1)}, bf16[128,128]{1,0:T(8,128)(2,1)}, u32[]{:S(2)}) copy-start(bf16[128,128]{1,0:T(8,128)(2,1)} %param.19) | copy-start | bytes 98308
  129.4 64.7 %copy-start.9 = (bf16[128,128]{1,0:T(8,128)(2,1)S(1)}, bf16[128,128]{1,0:T(8,128)(2,1)}, u32[]{:S(2)}) copy-start(bf16[128,128]{1,0:T(8,128)(2,1)} %param.20) | copy-start | bytes 98308
  129.5 66.0 %copy-start.15 = (f32[4]{0:T(128)S(1)}, f32[4]{0:T(128)}, u32[]{:S(2)}) copy-start(f32[4]{0:T(128)} %param.22) | copy-start | bytes 52
  129.5 148.7 %copy-start.6 = (bf16[128,256]{1,0:T(8,128)(2,1)S(1)}, bf16[128,256]{1,0:T(8,128)(2,1)}, u32[]{:S(2)}) copy-start(bf16[128,256]{1,0:T(8,128)(2,1)} %param.21) | copy-start | bytes 196612
  188.4 137.8 %all-to-all-start.1 = ((bf16[8,48,2048]{2,1,0:T(8,128)(2,1)}), bf16[8,48,2048]{2,1,0:T(8,128)(2,1)}, u32[]{:S(2)}, u32[]{:S(2)}) async-start(bf16[8,48,2048]{2,1,0:T(8,128)(2,1)} %bitcast.77), calls=%async_computation.3 | async-start | bytes 3145728 | tf_op jit(solution)/shard_map/all_to_all | solution.py:127
  193.9 149.9 %reduce-scatter.3.cloned.1.call-start = ((), (), s32[]{:S(2)}) async-start(), calls=%async_computation.4 | async-start | bytes 655360 | tf_op jit(solution)/shard_map/reduce_scatter | solution.py:89
  309.5 2.9 copy-start.7
  309.5 3.0 copy-start.4
  312.5 2.5 copy-start.1
  315.0 1.3 copy-start.3
  315.0 1.3 copy-start.11
  316.4 0.8 copy-start.5
  317.2 2.6 copy-start.2
  321.7 4.2 %copy-start.10 = (s32[128,2]{0,1:T(2,128)S(1)}, s32[128,2]{0,1:T(2,128)}, u32[]{:S(2)}) copy-start(s32[128,2]{0,1:T(2,128)} %param.27) | copy-start | bytes 3076
  321.7 4.4 %copy-start.14 = (f32[128,2]{0,1:T(2,128)S(1)}, f32[128,2]{0,1:T(2,128)}, u32[]{:S(2)}) copy-start(f32[128,2]{0,1:T(2,128)} %param.28) | copy-start | bytes 3076
  321.7 4.5 %copy-start.13 = (s32[256,1]{0,1:T(1,128)S(1)}, s32[256,1]{0,1:T(1,128)}, u32[]{:S(2)}) copy-start(s32[256,1]{0,1:T(1,128)} %copy-done.12) | copy-start | bytes 3076
Sparse Core Ops, SparseCore 0:
  63.6 45.3 all-gather.1
  129.6 58.8 reduce-scatter.4
  325.8 18.0 reduce-scatter.2
where the time goes:
time: 351 us; the launch traced here: 350 us
  blocking collectives  158 us (45%)
  waiting for transfers between devices  110 us (31%)
  matrix products  32.1 us (9%)
  local copies, waits for them, and re-layouts  16.1 us (5%)
  between operations  14.7 us (4%)
  other arithmetic  14 us (4%)
  starting transfers between devices  5.63 us (2%)
    reduce_scatter x1, waiting for transfers between devices, experts(): lax.psum_scatter(jnp.dot(hidden, w_down[0], preferred_element_type=jnp.fl...  58.9 us
    all_gather x1, blocking collectives, mixer(): piece_a = lax.all_gather(keys_a, 'ep', axis=0, tiled=True)  54.2 us
    all_gather x1, waiting for transfers between devices, experts(): lax.all_gather(arrived, 'tp', axis=0, tiled=True)  45.5 us
    all_to_all x1, blocking collectives, experts(): lax.all_to_all(outgoing, 'ep', split_axis=0, concat_axis=1, tiled=True)  44.2 us
    all_gather x1, blocking collectives, mixer(): piece_v = lax.all_gather(values, 'ep', axis=0, tiled=True)  31.3 us
    all_gather x1, blocking collectives, mixer(): piece_b = lax.all_gather(keys_b, 'ep', axis=0, tiled=True)  27.8 us
    dot_general x1, matrix products, experts(): jnp.dot(hidden, w_down[0], preferred_element_type=jnp.float32)  11.9 us
    dot_general x1, matrix products, hidden_rows(): gate = jnp.dot(inputs, gate_matrix, preferred_element_type=jnp.float32)  8.52 us
  transfers between devices with their start and end apart: 4, of which 3 were waited for; matrix products, arithmetic and copies ran while one was open for 8% of the time, Pallas kernels for 0%

commit v1 on v0

--- a/solution.py
+++ b/solution.py
@@ -10,6 +10,13 @@
 alpha_act = 1.702
 limit_act = 7.0
 negative = -1e30
+
+
+def trade_parts(shard, name, split, join):
+    n_dev = lax.axis_size(name)
+    blocks = jnp.stack(jnp.split(shard, n_dev, axis=split), axis=0)
+    blocks = lax.all_to_all(blocks, name, split_axis=0, concat_axis=0)
+    return jnp.concatenate(blocks, axis=join)
 
 
 def clamped_unit(gate, up):
@@ -114,9 +121,7 @@
         .set(jnp.arange(tok_rows * TOP, dtype=jnp.int32) // TOP)
     )
     outgoing = pick_rows(normed, owner).reshape(n_experts, capacity, width)
-    arrived = lax.all_to_all(outgoing, "ep", split_axis=0, concat_axis=1, tiled=True).reshape(
-        -1, width
-    )
+    arrived = trade_parts(outgoing, "ep", 0, 1).reshape(-1, width)
     hidden = hidden_rows(lax.all_gather(arrived, "tp", axis=0, tiled=True), w_gate[0], w_up[0])
     expert_out = lax.psum_scatter(
         jnp.dot(hidden, w_down[0], preferred_element_type=jnp.float32).astype(jnp.bfloat16),

time: 351 us -> 351 us (level)
  no operation moved by 1% of the time
where the time goes in v1:
time: 351 us; the launch traced here: 350 us
  blocking collectives  158 us (45%)
  waiting for transfers between devices  110 us (31%)
  matrix products  32.1 us (9%)
  local copies, waits for them, and re-layouts  16.1 us (5%)
  between operations  14.7 us (4%)
  other arithmetic  14 us (4%)
  starting transfers between devices  5.63 us (2%)
    reduce_scatter x1, waiting for transfers between devices, experts(): lax.psum_scatter(jnp.dot(hidden, w_down[0], preferred_element_type=jnp.fl...  59 us
    all_gather x1, blocking collectives, mixer(): piece_a = lax.all_gather(keys_a, 'ep', axis=0, tiled=True)  54.2 us
    all_gather x1, waiting for transfers between devices, experts(): lax.all_gather(arrived, 'tp', axis=0, tiled=True)  45.5 us
    all_to_all x1, blocking collectives, trade_parts(): blocks = lax.all_to_all(blocks, name, split_axis=0, concat_axis=0)  44.2 us
    all_gather x1, blocking collectives, mixer(): piece_v = lax.all_gather(values, 'ep', axis=0, tiled=True)  31.3 us
    all_gather x1, blocking collectives, mixer(): piece_b = lax.all_gather(keys_b, 'ep', axis=0, tiled=True)  27.8 us
    dot_general x1, matrix products, experts(): jnp.dot(hidden, w_down[0], preferred_element_type=jnp.float32)  11.9 us
    dot_general x1, matrix products, hidden_rows(): gate = jnp.dot(inputs, gate_matrix, preferred_element_type=jnp.float32)  8.52 us
  transfers between devices with their start and end apart: 4, of which 3 were waited for; matrix products, arithmetic and copies ran while one was open for 8% of the time, Pallas kernels for 0%

profile of v1, /device:TPU:0, one launch (start us, length us, event | category | flops | bytes accessed | tf_op | source)
XLA Modules:
  0.0 350.5 jit_solution(1431430407252617084)
XLA Ops:
  7.2 0.9 copy.49
  8.2 0.1 eq.26
  8.3 0.1 reshape.157
  8.4 0.7 broadcast_multiply_fusion
  9.1 0.6 reduce-window.6
  9.7 0.2 slice_reduce_fusion
  10.0 0.1 fusion.42
  10.1 0.1 copy.53
  10.2 0.1 mul.117
  10.3 1.4 scatter_custom_fusion
  11.8 1.2 fusion.27
  13.0 1.2 fusion.29
  14.3 3.1 gather_fusion
  17.4 1.7 select_select_fusion
  19.3 44.2 %all_to_all.10 = bf16[8,1,48,2048]{3,2,1,0:T(8,128)(2,1)} all-to-all(bf16[8,1,48,2048]{3,2,1,0:T(8,128)(2,1)S(1)} %fusion.32), channel_id=1, replica_groups=mesh['ep'=8,'tp'=4] {'ep'}, dimensions={0} | all-to-all | bytes 3145728 | tf_op jit(solution)/shard_map/all_to_all | solution.py:18
  63.6 45.5 %all-gather.2.cloned.1.call-done = bf16[1536,2048]{1,0:T(8,128)(2,1)} async-done(((bf16[384,2048]{1,0:T(8,128)(2,1)}), bf16[1536,2048]{1,0:T(8,128)(2,1)}) %all-gather.2.cloned.1.call-update) | async-done | bytes 6291472 | tf_op jit(solution)/shard_map/all_gather | solution.py:125
  109.0 8.5 %convolution_minimum_fusion = f32[1536,512]{1,0:T(8,128)} fusion(bf16[1536,2048]{1,0:T(8,128)(2,1)} %all-gather.2.cloned.1.call-done, bf16[1,2048,512]{2,1,0:T(8,128)(2,1)} %param.29), kind=kOutput, calls=%fused_computation.30 | convolution fusion | flops 3222011904 | bytes 11534336 | tf_op jit(solution)/shard_map/dot_general | solution.py:29
  117.6 11.9 %convolution_convert_fusion = bf16[1536,2048]{1,0:T(8,128)(2,1)} fusion(bf16[1,512,2048]{2,1,0:T(8,128)(2,1)S(1)} %copy-done, bf16[1536,2048]{1,0:T(8,128)(2,1)} %all-gather.2.cloned.1.call-done, f32[1536,512]{1,0:T(8,128)} %convolution_minimum_fusion, bf16[1,2048,512]{2,1,0:T(8,128)(2,1)} %param.30), kind=kOutput, calls=%fused_computation.28 | convolution fusion | flops 6452674560 | bytes 19922944 | tf_op jit(solution)/shard_map/dot_general | solution.py:127
  129.5 59.0 %reduce-scatter.5.cloned.1.call-done = bf16[384,2048]{1,0:T(8,128)(2,1)} async-done(((bf16[1536,2048]{1,0:T(8,128)(2,1)}), bf16[384,2048]{1,0:T(8,128)(2,1)}) %reduce-scatter.5.cloned.1.call-update) | async-done | bytes 1572880 | tf_op jit(solution)/shard_map/reduce_scatter | solution.py:126
  188.5 5.5 %all-to-all-start.1 = ((bf16[8,48,2048]{2,1,0:T(8,128)(2,1)}), bf16[8,48,2048]{2,1,0:T(8,128)(2,1)}, u32[]{:S(2)}, u32[]{:S(2)}) async-start(bf16[8,48,2048]{2,1,0:T(8,128)(2,1)} %bitcast.107), calls=%async_computation.3 | async-start | bytes 3145728 | tf_op jit(solution)/shard_map/all_to_all | solution.py:132
  194.0 0.1 copy.45
  194.2 0.1 copy.46
  194.3 0.6 slice.17
  195.6 0.7 mul.106
  196.2 54.2 %all_gather.12 = bf16[1024,128]{0,1:T(8,128)(2,1)S(1)} all-gather(bf16[128,128]{0,1:T(8,128)(2,1)S(1)} %copy.45), channel_id=1, replica_groups=mesh['ep'=8,'tp'=4] {'ep'}, dimensions={0}, use_global_device_ids=true | all-gather | bytes 294912 | tf_op jit(solution)/shard_map/all_gather | solution.py:71
  250.4 27.8 %all_gather.14 = bf16[1024,128]{0,1:T(8,128)(2,1)} all-gather(bf16[128,128]{0,1:T(8,128)(2,1)S(1)} %copy.46), channel_id=1, replica_groups=mesh['ep'=8,'tp'=4] {'ep'}, dimensions={0}, use_global_device_ids=true | all-gather | bytes 294912 | tf_op jit(solution)/shard_map/all_gather | solution.py:72
  278.2 31.3 %all_gather.13 = bf16[1024,256]{1,0:T(8,128)(2,1)S(1)} all-gather(bf16[128,256]{1,0:T(8,128)(2,1)S(1)} %copy-done.6), channel_id=1, replica_groups=mesh['ep'=8,'tp'=4] {'ep'}, dimensions={0}, use_global_device_ids=true | all-gather | bytes 589824 | tf_op jit(solution)/shard_map/all_gather | solution.py:73
  309.5 12.2 %conditional.1 = (f32[2,2,128]{2,1,0:T(2,128)S(1)}, f32[2,2,128,128]{3,2,1,0:T(8,128)S(1)}, f32[2,2,128]{2,1,0:T(2,128)S(1)}, f32[2,2,128,128]{3,2,1,0:T(8,128)S(1)}) conditional(s32[]{:T(128)} %bitcast.12, () %tuple.16, (s32[128]{0:T(128)S(1)}, bf16[1024,128]{0,1:T(8,128)(2,1)S(1)}, bf16[128,256]{1,0:T(8,128)(2,1)}, bf16[1024,256]{1,0:T(8,128)(2,1)S(1)}, ...), branch_computations={%region_0.0_spmd, %region_1.6_spmd} | conditional | flops 416414720 | bytes 47481572 | solution.py:88
  309.5 0.1 iota_compare_fusion
  309.6 1.0 copy.47
  310.6 1.8 fusion.50
  312.5 0.1 copy.48
  312.6 2.4 fusion.1
  315.0 1.0 fusion.5
  316.1 0.2 copy-done.3
  316.3 0.1 reshape.148
  316.4 0.8 copy-done.5
  317.2 2.6 fusion.6
  319.8 1.9 fusion.8
  321.8 1.0 multiply_reduce_fusion.1
  322.8 2.9 fusion.23
  325.7 0.1 sub.35
  326.0 0.1 copy.52
  326.1 0.1 copy.54
  326.3 4.0 %gather_fusion.1 = bf16[256,2048]{1,0:T(8,128)(2,1)S(1)} fusion(bf16[384,2048]{1,0:T(8,128)(2,1)} %bitcast.33, s32[1024]{0:T(1024)S(1)} %pad_clamp_fusion), kind=kCustom, calls=%fused_computation.1 | custom fusion | bytes 2098176 | tf_op jit(solution)/shard_map/jit(_take)/gather | solution.py:135
  330.3 1.5 gather.12
  331.8 6.2 %multiply_reduce_fusion = bf16[128,2048]{1,0:T(8,128)(2,1)} fusion(bf16[128,2,2048]{2,1,0:T(2,128)(2,1)} %gather.12, pred[128,2]{1,0:T(8,128)(4,1)S(1)} %copy.52, f32[128,2]{1,0:T(8,128)S(1)} %copy.54), kind=kLoop, calls=%fused_computation.39 | loop fusion | flops 1835008 | bytes 1574144 | tf_op jit(solution)/shard_map/reduce_sum | solution.py:136
  338.0 5.9 %reduce-scatter.3.cloned.1.call-done = bf16[32,2048]{1,0:T(8,128)(2,1)} async-done(((bf16[128,2048]{1,0:T(8,128)(2,1)}), bf16[32,2048]{1,0:T(8,128)(2,1)}) %reduce-scatter.3.cloned.1.call-update) | async-done | bytes 131088 | tf_op jit(solution)/shard_map/reduce_scatter | solution.py:96
  (61 shorter events, 0.6 us)
Async XLA Ops:
  7.2 110.4 %copy-start = (bf16[1,512,2048]{2,1,0:T(8,128)(2,1)S(1)}, bf16[1,512,2048]{2,1,0:T(8,128)(2,1)}, u32[]{:S(2)}) copy-start(bf16[1,512,2048]{2,1,0:T(8,128)(2,1)} %param.31) | copy-start | bytes 6291460
  7.2 101.8 %all-gather.2.cloned.1.call-start = ((), (), s32[]{:S(2)}) async-start(), calls=%async_computation.5 | async-start | bytes 7864320 | tf_op jit(solution)/shard_map/all_gather | solution.py:125
  10.3 1.4 copy-start.12
  63.5 125.0 %reduce-scatter.5.cloned.1.call-start = ((), (), s32[]{:S(2)}) async-start(), calls=%async_computation.6 | async-start | bytes 7864320 | tf_op jit(solution)/shard_map/reduce_scatter | solution.py:126
  129.4 64.6 %copy-start.8 = (bf16[128,128]{1,0:T(8,128)(2,1)S(1)}, bf16[128,128]{1,0:T(8,128)(2,1)}, u32[]{:S(2)}) copy-start(bf16[128,128]{1,0:T(8,128)(2,1)} %param.19) | copy-start | bytes 98308
  129.5 64.7 %copy-start.9 = (bf16[128,128]{1,0:T(8,128)(2,1)S(1)}, bf16[128,128]{1,0:T(8,128)(2,1)}, u32[]{:S(2)}) copy-start(bf16[128,128]{1,0:T(8,128)(2,1)} %param.20) | copy-start | bytes 98308
  129.5 66.1 %copy-start.15 = (f32[4]{0:T(128)S(1)}, f32[4]{0:T(128)}, u32[]{:S(2)}) copy-start(f32[4]{0:T(128)} %param.22) | copy-start | bytes 52
  129.5 148.7 %copy-start.6 = (bf16[128,256]{1,0:T(8,128)(2,1)S(1)}, bf16[128,256]{1,0:T(8,128)(2,1)}, u32[]{:S(2)}) copy-start(bf16[128,256]{1,0:T(8,128)(2,1)} %param.21) | copy-start | bytes 196612
  188.5 137.8 %all-to-all-start.1 = ((bf16[8,48,2048]{2,1,0:T(8,128)(2,1)}), bf16[8,48,2048]{2,1,0:T(8,128)(2,1)}, u32[]{:S(2)}, u32[]{:S(2)}) async-start(bf16[8,48,2048]{2,1,0:T(8,128)(2,1)} %bitcast.107), calls=%async_computation.3 | async-start | bytes 3145728 | tf_op jit(solution)/shard_map/all_to_all | solution.py:132
  194.0 149.9 %reduce-scatter.3.cloned.1.call-start = ((), (), s32[]{:S(2)}) async-start(), calls=%async_computation.4 | async-start | bytes 655360 | tf_op jit(solution)/shard_map/reduce_scatter | solution.py:96
  309.5 2.9 copy-start.7
  309.5 3.1 copy-start.4
  312.6 2.5 copy-start.1
  315.0 1.3 copy-start.3
  315.0 1.3 copy-start.11
  316.4 0.8 copy-start.5
  317.2 2.6 copy-start.2
  321.7 4.2 %copy-start.10 = (s32[128,2]{0,1:T(2,128)S(1)}, s32[128,2]{0,1:T(2,128)}, u32[]{:S(2)}) copy-start(s32[128,2]{0,1:T(2,128)} %param.27) | copy-start | bytes 3076
  321.8 4.4 %copy-start.14 = (f32[128,2]{0,1:T(2,128)S(1)}, f32[128,2]{0,1:T(2,128)}, u32[]{:S(2)}) copy-start(f32[128,2]{0,1:T(2,128)} %param.28) | copy-start | bytes 3076
  321.8 4.5 %copy-start.13 = (s32[256,1]{0,1:T(1,128)S(1)}, s32[256,1]{0,1:T(1,128)}, u32[]{:S(2)}) copy-start(s32[256,1]{0,1:T(1,128)} %copy-done.12) | copy-start | bytes 3076
Sparse Core Ops, SparseCore 0:
  63.6 45.3 all-gather.1
  129.6 58.8 reduce-scatter.4
  325.9 18.0 reduce-scatter.2
